TPU v7x, 256 devices: a 4x2x16 block of a 4x16x16 slice. The times are simulated.
256 devices in a mesh: grp: 2 (over y), fs: 16 (over z), tp: 8 (over x, core).
Axes of the slice: x: 4, y: 2, z: 16, core: 2. Of those that a mesh axis runs over, the one named last changes fastest.
The devices are a block of a 4x16x16 slice.
Arguments:
- tokens: bfloat16 [4096, 4096], P(('grp', 'tp')), parts along dimension 0, may hold values from -6 to 6
- routes: int32 [4096, 2], P(('grp', 'tp')), parts along dimension 0, may hold values from 0 to 7, all different within a row; in each aligned block of 256 rows (0 to 255, 256 to 511, ...) at most 128 rows name the same one
- route_weight: float32 [4096, 2], P(('grp', 'tp')), parts along dimension 0, may hold values from 0.2 to 1
- norm_gain: float32 [4096], P('fs'), may hold values from 0.1 to 1.9
- gate_train: float32 [8, 4096, 2048], P(None, 'fs', 'tp'), may hold values from -0.09375 to 0.09375
- up_train: float32 [8, 4096, 2048], P(None, 'fs', 'tp'), may hold values from -0.09375 to 0.09375
- down_train: float32 [8, 2048, 4096], P(None, 'fs', 'tp'), may hold values from -0.125 to 0.125
Outputs:
- gate_serve: bfloat16 [16, 4096, 2048], P(('grp', 'tp'), None, 'fs'), parts along dimension 0
- up_serve: bfloat16 [16, 4096, 2048], P(('grp', 'tp'), None, 'fs'), parts along dimension 0
- down_serve: bfloat16 [16, 2048, 4096], P(('grp', 'tp'), 'fs'), parts along dimension 0
- moe_out: bfloat16 [4096, 4096], P(('grp', 'tp'), 'fs'), parts along dimension 0
There are 2 independent parts, one for each index of `grp`. A program takes and returns all parts, laid end to end along the dimension named above; an argument that names none is the same for every part. Nothing has to cross between parts.
Inputs may be any that keep to these rules, and one draw needn't show every extreme that they name: `routes`: within the 256 rows of each device (aligned blocks), no expert is named by more than 128 rows, a bound that some block reaches; the two experts of a row differ; every expert is named somewhere.
All inputs are finite; a program needn't handle non-finite values.
Results may differ from a plain program's by a relative error of at most 0.0076.
Values may be sent and summed in bfloat16 or wider, within the bound.
No kernel may reach another device: no remote copies, remote signals or barrier semaphores. Data moves between devices by JAX's collectives and lax.ppermute only.
A program may use at most 128 MiB of HBM per device.

v0:
```python
import jax
import jax.numpy as jnp
from jax import lax
from jax.sharding import PartitionSpec as P

EXPERTS = 8
CAP = 128


def side_by_side(arrays, axis, split_dim, concat_dim, along):
    both = jnp.concatenate(arrays, axis=along)
    filled, at, gathered = (
        lax.all_to_all(both, axis, split_axis=split_dim, concat_axis=concat_dim, tiled=True),
        0,
        [],
    )
    for a in arrays:
        gathered.append(lax.slice_in_dim(filled, at, at + a.shape[along], axis=along))
        at += a.shape[along]
    return tuple(gathered)


def split_up(value, dim, length):
    lengths = value.shape
    tiles = value.reshape(*lengths[:dim], length, lengths[dim] // length, *lengths[dim + 1 :])
    return jnp.moveaxis(tiles, dim, 0)


def cut_rows(length, count):
    turn = length // count
    if turn >= 8:
        turn -= turn % 8
    return [turn * k for k in range(1, count)]


def laid_out(tiles, dim):
    lengths = list(tiles.shape[1:])
    lengths[dim] *= tiles.shape[0]
    return jnp.moveaxis(tiles, 0, dim).reshape(lengths)


def exchange_in_pieces(value, axis, pieces, split_dim, concat_dim):
    tiles = split_up(value, split_dim, lax.axis_size(axis))
    cut = max(range(1, max(2, tiles.ndim - 1)), key=lambda d: tiles.shape[d])
    gathered = []
    for slab in jnp.split(tiles, cut_rows(tiles.shape[cut], pieces), axis=cut):
        if slab.size:
            gathered.append(lax.all_to_all(slab, axis, split_axis=0, concat_axis=0, tiled=True))
    return laid_out(jnp.concatenate(gathered, axis=cut), concat_dim)


def per_device(tokens, routes, route_weight, norm_gain, gate_train, up_train, down_train):
    gate_cast = (norm_gain[None, :, None] * gate_train).astype(jnp.bfloat16)
    up_cast = (norm_gain[None, :, None] * up_train).astype(jnp.bfloat16)
    down_cast = down_train.astype(jnp.bfloat16)
    gate_mid, up_mid, down_serve = (
        *side_by_side((gate_cast, up_cast), "tp", 0, 2, 1),
        lax.all_to_all(down_cast, "tp", split_axis=0, concat_axis=2, tiled=True),
    )
    gate_serve, up_serve = side_by_side((gate_mid, up_mid), "fs", 2, 1, 0)
    tok_rows = tokens.shape[0]
    flat = routes.reshape(-1)
    expert_ids = jnp.arange(EXPERTS, dtype=jnp.int32)
    onehot = (flat[:, None] == expert_ids[None, :]).astype(jnp.int32)
    before = jnp.cumsum(onehot, axis=0) - onehot
    slot = jnp.sum(before * onehot, axis=1)
    place = (flat * CAP + slot).reshape(tok_rows, 2)
    slot_ids = jnp.arange(EXPERTS * CAP, dtype=jnp.int32)
    select = jnp.any(place[None, :, :] == slot_ids[:, None, None], axis=2).astype(jnp.bfloat16)
    outgoing = jnp.dot(select, tokens, preferred_element_type=jnp.float32).astype(jnp.bfloat16)
    arrived = lax.all_to_all(outgoing, "tp", split_axis=0, concat_axis=0, tiled=True)
    senders = lax.axis_size("tp")
    local = gate_serve.shape[0]
    arrived = arrived.reshape(senders, local, CAP, arrived.shape[1])
    gate_h = jnp.einsum("tlcd,ldf->tlcf", arrived, gate_serve, preferred_element_type=jnp.float32)
    up_h = jnp.einsum("tlcd,ldf->tlcf", arrived, up_serve, preferred_element_type=jnp.float32)
    hidden = (jax.nn.silu(gate_h) * up_h).astype(jnp.bfloat16)
    down_cols = exchange_in_pieces(down_serve, "fs", 2, 2, 1)
    empty = jnp.zeros((down_cols.shape[2], senders * local * CAP), jnp.float32)
    term = jnp.einsum(
        "tlcf,lfd->dtlc",
        lax.all_gather(hidden, "fs", axis=3, tiled=True),
        down_cols,
        preferred_element_type=jnp.float32,
    )
    summed = term.reshape(empty.shape)
    returned = lax.all_to_all(
        summed.astype(jnp.bfloat16), "tp", split_axis=1, concat_axis=1, tiled=True
    )
    picked = jnp.take(returned, place, axis=1)
    mixed = (
        picked[:, :, 0].astype(jnp.float32) * route_weight[None, :, 0]
        + picked[:, :, 1].astype(jnp.float32) * route_weight[None, :, 1]
    )
    moe_out = mixed.T.astype(jnp.bfloat16)
    return (gate_serve, up_serve, down_serve, moe_out)


def solution(mesh):
    return jax.shard_map(
        per_device,
        mesh=mesh,
        in_specs=(
            P(("grp", "tp"), None),
            P(("grp", "tp"), None),
            P(("grp", "tp"), None),
            P("fs"),
            P(None, "fs", "tp"),
            P(None, "fs", "tp"),
            P(None, "fs", "tp"),
        ),
        out_specs=(
            P(("grp", "tp"), None, "fs"),
            P(("grp", "tp"), None, "fs"),
            P(("grp", "tp"), "fs", None),
            P(("grp", "tp"), "fs"),
        ),
        check_vma=False,
    )
```

profile of v0, /device:TPU:33, one launch (start us, length us, event | category | flops | bytes accessed | tf_op | source)
XLA Modules:
  0.0 444.2 jit_solution(10201780460128886947)
XLA Ops:
  7.2 3.1 copy.96
  10.3 2.9 copy.97
  13.2 2.6 multiply_convert_fusion.1
  16.0 49.1 %all_to_all.82 = bf16[8,512,256]{1,2,0:T(8,128)(2,1)S(1)} all-to-all(bf16[8,512,256]{1,2,0:T(8,128)(2,1)S(1)} %pad_maximum_fusion), channel_id=1, replica_groups=mesh['grp'=2,'fs'=16,'tp'=8] {'tp'}, dimensions={0} | all-to-all | bytes 4194304 | tf_op jit(solution)/shard_map/all_to_all | solution.py:13
  65.5 14.0 %copy.98 = bf16[2,256,2048]{1,0,2:T(2,128)(2,1)} copy(bf16[2,256,2048]{1,2,0:T(8,128)(2,1)S(1)} %pad_maximum_fusion.1) | data formatting | bytes 4194304 | tf_op jit(solution)/shard_map/concatenate | solution.py:11
  79.5 6.7 %all-to-all-start.1 = ((bf16[2,256,2048]{1,0,2:T(2,128)(2,1)}), bf16[2,256,2048]{1,0,2:T(2,128)(2,1)}, u32[]{:S(2)}, u32[]{:S(2)}) async-start(bf16[2,256,2048]{1,0,2:T(2,128)(2,1)} %copy.98), calls=%async_computation.1 | async-start | bytes 4194304 | tf_op jit(solution)/shard_map/all_to_all | solution.py:13
  88.8 5.6 %convolution_convert_fusion = bf16[1024,4096]{1,0:T(8,128)(2,1)} fusion(pred[1024,256]{1,0:T(8,128)(4,1)S(1)} %fusion, bf16[256,4096]{1,0:T(8,128)(2,1)S(1)} %copy-done), kind=kOutput, calls=%fused_computation.1 | convolution fusion | flops 2151677952 | bytes 10747904 | tf_op jit(solution)/shard_map/dot_general | solution.py:70
  94.4 83.6 %all-to-all-done.1 = bf16[2,256,2048]{1,0,2:T(2,128)(2,1)} async-done(((bf16[2,256,2048]{1,0,2:T(2,128)(2,1)}), bf16[2,256,2048]{1,0,2:T(2,128)(2,1)}, u32[]{:S(2)}, u32[]{:S(2)}) %all-to-all-start.1) | async-done | bytes 2097184 | tf_op jit(solution)/shard_map/all_to_all | solution.py:13
  178.0 9.5 %all-to-all-start.5 = ((bf16[8,128,4096]{2,1,0:T(8,128)(2,1)}), bf16[8,128,4096]{2,1,0:T(8,128)(2,1)}, u32[]{:S(2)}, u32[]{:S(2)}) async-start(bf16[8,128,4096]{2,1,0:T(8,128)(2,1)} %bitcast.83), calls=%async_computation.5 | async-start | bytes 16777216 | tf_op jit(solution)/shard_map/all_to_all | solution.py:71
  187.5 1.9 copy.99
  189.5 1.6 copy.110
  191.1 1.6 reshape.98
  192.6 1.6 copy.111
  194.2 2.3 reshape.99
  196.5 84.8 %all-to-all-done.5 = bf16[8,128,4096]{2,1,0:T(8,128)(2,1)} async-done(((bf16[8,128,4096]{2,1,0:T(8,128)(2,1)}), bf16[8,128,4096]{2,1,0:T(8,128)(2,1)}, u32[]{:S(2)}, u32[]{:S(2)}) %all-to-all-start.5) | async-done | bytes 8388640 | tf_op jit(solution)/shard_map/all_to_all | solution.py:71
  281.3 6.3 %convolution_bitcast_fusion.1 = f32[8,1,128,128]{2,3,0,1:T(8,128)S(1)} fusion(bf16[4096,128,1]{0,1,2:T(8,128)(2,1)S(1)} %reshape.98, bf16[8,128,4096]{2,1,0:T(8,128)(2,1)} %all-to-all-done.5), kind=kOutput, calls=%fused_computation.12 | convolution fusion | flops 1073741824 | bytes 9961472 | tf_op jit(solution)/shard_map/tlcd,ldf->tlcf/dot_general | solution.py:75
  287.7 7.1 %fusion.3 = bf16[8,1,128,128]{2,3,0,1:T(8,128)(2,1)} fusion(bf16[4096,128,1]{0,1,2:T(8,128)(2,1)S(1)} %copy-done.2, bf16[8,128,4096]{2,1,0:T(8,128)(2,1)} %all-to-all-done.5, f32[8,1,128,128]{2,3,0,1:T(8,128)S(1)} %convolution_bitcast_fusion.1), kind=kOutput, calls=%fused_computation.13 | convolution fusion | flops 1074528256 | bytes 10223616 | tf_op jit(solution)/shard_map/tlcd,ldf->tlcf/dot_general | solution.py:76
  294.8 2.5 copy.102
  297.4 19.4 %all_to_all.83 = bf16[8,128,512]{1,2,0:T(8,128)(2,1)S(1)} all-to-all(bf16[8,128,512]{1,2,0:T(8,128)(2,1)} %copy.102), channel_id=1, replica_groups=mesh['grp'=2,'fs'=16,'tp'=8] {'tp'}, dimensions={0} | all-to-all | bytes 2097152 | tf_op jit(solution)/shard_map/all_to_all | solution.py:58
  316.8 1.7 fusion.13
  318.5 2.4 copy.106
  320.9 7.1 %all-to-all-start.3 = ((bf16[16,1,64,256]{3,2,1,0:T(8,128)(2,1)}), bf16[16,1,64,256]{3,2,1,0:T(8,128)(2,1)}, u32[]{:S(2)}, u32[]{:S(2)}) async-start(bf16[16,1,64,256]{3,2,1,0:T(8,128)(2,1)} %copy.106), calls=%async_computation.3 | async-start | bytes 1048576 | tf_op jit(solution)/shard_map/all_to_all | solution.py:48
  328.0 2.4 copy.107
  330.4 27.1 %all-to-all-done.3 = bf16[16,1,64,256]{3,2,1,0:T(8,128)(2,1)} async-done(((bf16[16,1,64,256]{3,2,1,0:T(8,128)(2,1)}), bf16[16,1,64,256]{3,2,1,0:T(8,128)(2,1)}, u32[]{:S(2)}, u32[]{:S(2)}) %all-to-all-start.3) | async-done | bytes 524320 | tf_op jit(solution)/shard_map/all_to_all | solution.py:48
  357.5 40.3 %all_to_all.84 = bf16[16,1,64,256]{3,2,1,0:T(8,128)(2,1)S(1)} all-to-all(bf16[16,1,64,256]{3,2,1,0:T(8,128)(2,1)} %copy.107), channel_id=1, replica_groups=mesh['grp'=2,'fs'=16,'tp'=8] {'fs'}, dimensions={0} | all-to-all | bytes 1048576 | tf_op jit(solution)/shard_map/all_to_all | solution.py:48
  397.8 2.1 pad_maximum_fusion.2
  400.6 6.5 %copy.112 = bf16[8,1,128,2048]{3,2,0,1:T(8,128)(2,1)} copy(bf16[8,1,128,2048]{2,3,0,1:T(8,128)(2,1)} %all-gather.2.cloned.1.call-done) | data formatting | bytes 8388608 | tf_op jit(solution)/shard_map/all_gather | solution.py:82
  407.1 3.8 fusion.1
  411.8 11.8 %all-to-all-start.6 = ((bf16[256,8,128]{2,0,1:T(8,128)(2,1)}), bf16[256,8,128]{2,0,1:T(8,128)(2,1)}, u32[]{:S(2)}, u32[]{:S(2)}) async-start(bf16[256,8,128]{2,0,1:T(8,128)(2,1)} %bitcast.89), calls=%async_computation.6 | async-start | bytes 1048576 | tf_op jit(solution)/shard_map/all_to_all | solution.py:87
  424.0 1.3 copy.117
  427.9 5.2 %all-to-all-done.6 = bf16[256,8,128]{2,0,1:T(8,128)(2,1)} async-done(((bf16[256,8,128]{2,0,1:T(8,128)(2,1)}), bf16[256,8,128]{2,0,1:T(8,128)(2,1)}, u32[]{:S(2)}, u32[]{:S(2)}) %all-to-all-start.6) | async-done | bytes 524320 | tf_op jit(solution)/shard_map/all_to_all | solution.py:87
  434.4 2.0 gather_fusion
  (44 shorter events, 10.0 us)
Async XLA Ops:
  7.2 81.6 %copy-start = (bf16[256,4096]{1,0:T(8,128)(2,1)S(1)}, bf16[256,4096]{1,0:T(8,128)(2,1)}, u32[]{:S(2)}) copy-start(bf16[256,4096]{1,0:T(8,128)(2,1)} %param.7) | copy-start | bytes 6291460
  10.3 2.9 copy-start.5
  79.5 6.7 %copy-start.3 = (s32[256,2]{0,1:T(2,128)S(1)}, s32[256,2]{0,1:T(2,128)}, u32[]{:S(2)}) copy-start(s32[256,2]{0,1:T(2,128)} %param.8) | copy-start | bytes 6148
  79.5 98.5 %all-to-all-start.1 = ((bf16[2,256,2048]{1,0,2:T(2,128)(2,1)}), bf16[2,256,2048]{1,0,2:T(2,128)(2,1)}, u32[]{:S(2)}, u32[]{:S(2)}) async-start(bf16[2,256,2048]{1,0,2:T(2,128)(2,1)} %copy.98), calls=%async_computation.1 | async-start | bytes 4194304 | tf_op jit(solution)/shard_map/all_to_all | solution.py:13
  178.0 103.3 %all-to-all-start.5 = ((bf16[8,128,4096]{2,1,0:T(8,128)(2,1)}), bf16[8,128,4096]{2,1,0:T(8,128)(2,1)}, u32[]{:S(2)}, u32[]{:S(2)}) async-start(bf16[8,128,4096]{2,1,0:T(8,128)(2,1)} %bitcast.83), calls=%async_computation.5 | async-start | bytes 16777216 | tf_op jit(solution)/shard_map/all_to_all | solution.py:71
  187.5 213.1 %all-gather.2.cloned.1.call-start = ((), (), s32[]{:S(2)}) async-start(), calls=%async_computation.7 | async-start | bytes 4456448 | tf_op jit(solution)/shard_map/all_gather | solution.py:82
  281.3 6.4 %copy-start.2 = (bf16[4096,128,1]{0,1,2:T(8,128)(2,1)S(1)}, bf16[4096,128,1]{0,1,2:T(8,128)(2,1)}, u32[]{:S(2)}) copy-start(bf16[4096,128,1]{0,1,2:T(8,128)(2,1)} %reshape.99) | copy-start | bytes 3145732
  320.9 36.6 %all-to-all-start.3 = ((bf16[16,1,64,256]{3,2,1,0:T(8,128)(2,1)}), bf16[16,1,64,256]{3,2,1,0:T(8,128)(2,1)}, u32[]{:S(2)}, u32[]{:S(2)}) async-start(bf16[16,1,64,256]{3,2,1,0:T(8,128)(2,1)} %copy.106), calls=%async_computation.3 | async-start | bytes 1048576 | tf_op jit(solution)/shard_map/all_to_all | solution.py:48
  410.9 13.1 %copy-start.4 = (f32[256,2]{0,1:T(2,128)S(1)}, f32[256,2]{0,1:T(2,128)}, u32[]{:S(2)}) copy-start(f32[256,2]{0,1:T(2,128)} %param.9) | copy-start | bytes 6148
  411.8 21.3 %all-to-all-start.6 = ((bf16[256,8,128]{2,0,1:T(8,128)(2,1)}), bf16[256,8,128]{2,0,1:T(8,128)(2,1)}, u32[]{:S(2)}, u32[]{:S(2)}) async-start(bf16[256,8,128]{2,0,1:T(8,128)(2,1)} %bitcast.89), calls=%async_computation.6 | async-start | bytes 1048576 | tf_op jit(solution)/shard_map/all_to_all | solution.py:87
  434.4 3.0 copy-start.1
Sparse Core Ops, SparseCore 0:
  294.9 105.5 all-gather.1
where the time goes:
time: 445 us; the launch traced here: 444 us
  waiting for transfers between devices  202 us (45%)
  blocking collectives  109 us (24%)
  local copies, waits for them, and re-layouts  53.9 us (12%)
  starting transfers between devices  35.2 us (8%)
  matrix products  22.8 us (5%)
  between operations  14.3 us (3%)
  other arithmetic  7.73 us (2%)
    all_to_all x1, waiting for transfers between devices, per_device(): lax.all_to_all(outgoing, 'tp', split_axis=0, concat_axis=0, tiled=True)  84.8 us
    all_to_all x1, waiting for transfers between devices, side_by_side(): lax.all_to_all(both, axis, split_axis=split_dim, concat_axis=concat_dim,...  83.6 us
    all_to_all x1, blocking collectives, side_by_side(): lax.all_to_all(both, axis, split_axis=split_dim, concat_axis=concat_dim,...  49.1 us
    all_to_all x1, blocking collectives, exchange_in_pieces(): lax.all_to_all(slab, axis, split_axis=0, concat_axis=0, tiled=True)  40.3 us
    all_to_all x1, waiting for transfers between devices, exchange_in_pieces(): lax.all_to_all(slab, axis, split_axis=0, concat_axis=0, tiled=True)  27.1 us
    all_to_all x1, blocking collectives, per_device(): lax.all_to_all(down_cast, 'tp', split_axis=0, concat_axis=2, tiled=True)  19.4 us
    concatenate x1, local copies, waits for them, and re-layouts, side_by_side(): both = jnp.concatenate(arrays, axis=along)  14 us
    all_to_all x1, starting transfers between devices, per_device(): lax.all_to_all(summed.astype(jnp.bfloat16), 'tp', split_axis=1, concat_ax...  11.8 us
  transfers between devices with their start and end apart: 5, of which 5 were waited for; matrix products, arithmetic and copies ran while one was open for 7% of the time, Pallas kernels for 0%

commit v1 on v0

--- a/solution.py
+++ b/solution.py
@@ -84,8 +84,14 @@
         preferred_element_type=jnp.float32,
     )
     summed = term.reshape(empty.shape)
-    returned = lax.all_to_all(
-        summed.astype(jnp.bfloat16), "tp", split_axis=1, concat_axis=1, tiled=True
+    returned = jnp.concatenate(
+        lax.all_to_all(
+            jnp.stack(jnp.split(summed.astype(jnp.bfloat16), lax.axis_size("tp"), axis=1)),
+            "tp",
+            0,
+            0,
+        ),
+        axis=1,
     )
     picked = jnp.take(returned, place, axis=1)
     mixed = (

time: 445 us -> 450 us (1.011)
    unnamed x17 -> x24, local copies, waits for them, and re-layouts: 10 us -> 14.5 us
where the time goes in v1:
time: 450 us; the launch traced here: 449 us
  waiting for transfers between devices  202 us (45%)
  blocking collectives  109 us (24%)
  local copies, waits for them, and re-layouts  58.2 us (13%)
  starting transfers between devices  35.2 us (8%)
  matrix products  22.8 us (5%)
  between operations  14.3 us (3%)
  other arithmetic  7.73 us (2%)
    all_to_all x1, waiting for transfers between devices, per_device(): lax.all_to_all(outgoing, 'tp', split_axis=0, concat_axis=0, tiled=True)  84.8 us
    all_to_all x1, waiting for transfers between devices, side_by_side(): lax.all_to_all(both, axis, split_axis=split_dim, concat_axis=concat_dim,...  83.6 us
    all_to_all x1, blocking collectives, side_by_side(): lax.all_to_all(both, axis, split_axis=split_dim, concat_axis=concat_dim,...  49.1 us
    all_to_all x1, blocking collectives, exchange_in_pieces(): lax.all_to_all(slab, axis, split_axis=0, concat_axis=0, tiled=True)  40.3 us
    all_to_all x1, waiting for transfers between devices, exchange_in_pieces(): lax.all_to_all(slab, axis, split_axis=0, concat_axis=0, tiled=True)  27.1 us
    all_to_all x1, blocking collectives, per_device(): lax.all_to_all(down_cast, 'tp', split_axis=0, concat_axis=2, tiled=True)  19.4 us
    unnamed x24, local copies, waits for them, and re-layouts  14.5 us
    concatenate x1, local copies, waits for them, and re-layouts, side_by_side(): both = jnp.concatenate(arrays, axis=along)  14 us
  transfers between devices with their start and end apart: 5, of which 5 were waited for; matrix products, arithmetic and copies ran while one was open for 7% of the time, Pallas kernels for 0%

profile of v1, /device:TPU:33, one launch (start us, length us, event | category | flops | bytes accessed | tf_op | source)
XLA Modules:
  0.0 448.5 jit_solution(4103921136115488898)
XLA Ops:
  7.2 3.1 copy.93
  10.3 2.9 copy.94
  13.2 2.6 multiply_convert_fusion.1
  16.0 49.1 %all_to_all.75 = bf16[8,512,256]{1,2,0:T(8,128)(2,1)S(1)} all-to-all(bf16[8,512,256]{1,2,0:T(8,128)(2,1)S(1)} %pad_maximum_fusion), channel_id=1, replica_groups=mesh['grp'=2,'fs'=16,'tp'=8] {'tp'}, dimensions={0} | all-to-all | bytes 4194304 | tf_op jit(solution)/shard_map/all_to_all | solution.py:13
  65.5 14.0 %copy.95 = bf16[2,256,2048]{1,0,2:T(2,128)(2,1)} copy(bf16[2,256,2048]{1,2,0:T(8,128)(2,1)S(1)} %pad_maximum_fusion.1) | data formatting | bytes 4194304 | tf_op jit(solution)/shard_map/concatenate | solution.py:11
  79.5 6.7 %all-to-all-start.1 = ((bf16[2,256,2048]{1,0,2:T(2,128)(2,1)}), bf16[2,256,2048]{1,0,2:T(2,128)(2,1)}, u32[]{:S(2)}, u32[]{:S(2)}) async-start(bf16[2,256,2048]{1,0,2:T(2,128)(2,1)} %copy.95), calls=%async_computation.1 | async-start | bytes 4194304 | tf_op jit(solution)/shard_map/all_to_all | solution.py:13
  88.8 5.6 %convolution_convert_fusion = bf16[1024,4096]{1,0:T(8,128)(2,1)} fusion(pred[1024,256]{1,0:T(8,128)(4,1)S(1)} %fusion, bf16[256,4096]{1,0:T(8,128)(2,1)S(1)} %copy-done), kind=kOutput, calls=%fused_computation.1 | convolution fusion | flops 2151677952 | bytes 10747904 | tf_op jit(solution)/shard_map/dot_general | solution.py:70
  94.4 83.6 %all-to-all-done.1 = bf16[2,256,2048]{1,0,2:T(2,128)(2,1)} async-done(((bf16[2,256,2048]{1,0,2:T(2,128)(2,1)}), bf16[2,256,2048]{1,0,2:T(2,128)(2,1)}, u32[]{:S(2)}, u32[]{:S(2)}) %all-to-all-start.1) | async-done | bytes 2097184 | tf_op jit(solution)/shard_map/all_to_all | solution.py:13
  178.0 9.5 %all-to-all-start.5 = ((bf16[8,128,4096]{2,1,0:T(8,128)(2,1)}), bf16[8,128,4096]{2,1,0:T(8,128)(2,1)}, u32[]{:S(2)}, u32[]{:S(2)}) async-start(bf16[8,128,4096]{2,1,0:T(8,128)(2,1)} %bitcast.111), calls=%async_computation.5 | async-start | bytes 16777216 | tf_op jit(solution)/shard_map/all_to_all | solution.py:71
  187.5 1.9 copy.96
  189.5 1.6 copy.107
  191.1 1.6 reshape.104
  192.6 1.6 copy.108
  194.2 2.3 reshape.105
  196.5 84.8 %all-to-all-done.5 = bf16[8,128,4096]{2,1,0:T(8,128)(2,1)} async-done(((bf16[8,128,4096]{2,1,0:T(8,128)(2,1)}), bf16[8,128,4096]{2,1,0:T(8,128)(2,1)}, u32[]{:S(2)}, u32[]{:S(2)}) %all-to-all-start.5) | async-done | bytes 8388640 | tf_op jit(solution)/shard_map/all_to_all | solution.py:71
  281.3 6.3 %convolution_bitcast_fusion.1 = f32[8,1,128,128]{2,3,0,1:T(8,128)S(1)} fusion(bf16[4096,128,1]{0,1,2:T(8,128)(2,1)S(1)} %reshape.104, bf16[8,128,4096]{2,1,0:T(8,128)(2,1)} %all-to-all-done.5), kind=kOutput, calls=%fused_computation.11 | convolution fusion | flops 1073741824 | bytes 9961472 | tf_op jit(solution)/shard_map/tlcd,ldf->tlcf/dot_general | solution.py:75
  287.7 7.1 %fusion.2 = bf16[8,1,128,128]{2,3,0,1:T(8,128)(2,1)} fusion(bf16[4096,128,1]{0,1,2:T(8,128)(2,1)S(1)} %copy-done.2, bf16[8,128,4096]{2,1,0:T(8,128)(2,1)} %all-to-all-done.5, f32[8,1,128,128]{2,3,0,1:T(8,128)S(1)} %convolution_bitcast_fusion.1), kind=kOutput, calls=%fused_computation.12 | convolution fusion | flops 1074528256 | bytes 10223616 | tf_op jit(solution)/shard_map/tlcd,ldf->tlcf/dot_general | solution.py:76
  294.8 2.5 copy.99
  297.4 19.4 %all_to_all.76 = bf16[8,128,512]{1,2,0:T(8,128)(2,1)S(1)} all-to-all(bf16[8,128,512]{1,2,0:T(8,128)(2,1)} %copy.99), channel_id=1, replica_groups=mesh['grp'=2,'fs'=16,'tp'=8] {'tp'}, dimensions={0} | all-to-all | bytes 2097152 | tf_op jit(solution)/shard_map/all_to_all | solution.py:58
  316.8 1.7 fusion.20
  318.5 2.4 copy.103
  320.9 7.1 %all-to-all-start.3 = ((bf16[16,1,64,256]{3,2,1,0:T(8,128)(2,1)}), bf16[16,1,64,256]{3,2,1,0:T(8,128)(2,1)}, u32[]{:S(2)}, u32[]{:S(2)}) async-start(bf16[16,1,64,256]{3,2,1,0:T(8,128)(2,1)} %copy.103), calls=%async_computation.3 | async-start | bytes 1048576 | tf_op jit(solution)/shard_map/all_to_all | solution.py:48
  328.0 2.4 copy.104
  330.4 27.1 %all-to-all-done.3 = bf16[16,1,64,256]{3,2,1,0:T(8,128)(2,1)} async-done(((bf16[16,1,64,256]{3,2,1,0:T(8,128)(2,1)}), bf16[16,1,64,256]{3,2,1,0:T(8,128)(2,1)}, u32[]{:S(2)}, u32[]{:S(2)}) %all-to-all-start.3) | async-done | bytes 524320 | tf_op jit(solution)/shard_map/all_to_all | solution.py:48
  357.5 40.3 %all_to_all.77 = bf16[16,1,64,256]{3,2,1,0:T(8,128)(2,1)S(1)} all-to-all(bf16[16,1,64,256]{3,2,1,0:T(8,128)(2,1)} %copy.104), channel_id=1, replica_groups=mesh['grp'=2,'fs'=16,'tp'=8] {'fs'}, dimensions={0} | all-to-all | bytes 1048576 | tf_op jit(solution)/shard_map/all_to_all | solution.py:48
  397.8 2.1 pad_maximum_fusion.2
  400.6 6.5 %copy.109 = bf16[8,1,128,2048]{3,2,0,1:T(8,128)(2,1)} copy(bf16[8,1,128,2048]{2,3,0,1:T(8,128)(2,1)} %all-gather.2.cloned.1.call-done) | data formatting | bytes 8388608 | tf_op jit(solution)/shard_map/all_gather | solution.py:82
  407.1 3.8 convolution_convert_fusion.1
  416.1 11.8 %all-to-all-start.6 = ((bf16[8,256,128]{2,1,0:T(8,128)(2,1)}), bf16[8,256,128]{2,1,0:T(8,128)(2,1)}, u32[]{:S(2)}, u32[]{:S(2)}) async-start(bf16[8,256,128]{2,1,0:T(8,128)(2,1)} %fusion.7), calls=%async_computation.6 | async-start | bytes 1048576 | tf_op jit(solution)/shard_map/all_to_all | solution.py:88
  428.3 1.3 copy.113
  432.2 5.2 %all-to-all-done.6 = bf16[8,256,128]{2,1,0:T(8,128)(2,1)} async-done(((bf16[8,256,128]{2,1,0:T(8,128)(2,1)}), bf16[8,256,128]{2,1,0:T(8,128)(2,1)}, u32[]{:S(2)}, u32[]{:S(2)}) %all-to-all-start.6) | async-done | bytes 524320 | tf_op jit(solution)/shard_map/all_to_all | solution.py:88
  438.6 2.0 gather_fusion
  (51 shorter events, 14.3 us)
Async XLA Ops:
  7.2 81.6 %copy-start = (bf16[256,4096]{1,0:T(8,128)(2,1)S(1)}, bf16[256,4096]{1,0:T(8,128)(2,1)}, u32[]{:S(2)}) copy-start(bf16[256,4096]{1,0:T(8,128)(2,1)} %param.7) | copy-start | bytes 6291460
  10.3 2.9 copy-start.5
  79.5 6.7 %copy-start.3 = (s32[256,2]{0,1:T(2,128)S(1)}, s32[256,2]{0,1:T(2,128)}, u32[]{:S(2)}) copy-start(s32[256,2]{0,1:T(2,128)} %param.8) | copy-start | bytes 6148
  79.5 98.5 %all-to-all-start.1 = ((bf16[2,256,2048]{1,0,2:T(2,128)(2,1)}), bf16[2,256,2048]{1,0,2:T(2,128)(2,1)}, u32[]{:S(2)}, u32[]{:S(2)}) async-start(bf16[2,256,2048]{1,0,2:T(2,128)(2,1)} %copy.95), calls=%async_computation.1 | async-start | bytes 4194304 | tf_op jit(solution)/shard_map/all_to_all | solution.py:13
  178.0 103.3 %all-to-all-start.5 = ((bf16[8,128,4096]{2,1,0:T(8,128)(2,1)}), bf16[8,128,4096]{2,1,0:T(8,128)(2,1)}, u32[]{:S(2)}, u32[]{:S(2)}) async-start(bf16[8,128,4096]{2,1,0:T(8,128)(2,1)} %bitcast.111), calls=%async_computation.5 | async-start | bytes 16777216 | tf_op jit(solution)/shard_map/all_to_all | solution.py:71
  187.5 213.1 %all-gather.2.cloned.1.call-start = ((), (), s32[]{:S(2)}) async-start(), calls=%async_computation.7 | async-start | bytes 4456448 | tf_op jit(solution)/shard_map/all_gather | solution.py:82
  281.3 6.4 %copy-start.2 = (bf16[4096,128,1]{0,1,2:T(8,128)(2,1)S(1)}, bf16[4096,128,1]{0,1,2:T(8,128)(2,1)}, u32[]{:S(2)}) copy-start(bf16[4096,128,1]{0,1,2:T(8,128)(2,1)} %reshape.105) | copy-start | bytes 3145732
  320.9 36.6 %all-to-all-start.3 = ((bf16[16,1,64,256]{3,2,1,0:T(8,128)(2,1)}), bf16[16,1,64,256]{3,2,1,0:T(8,128)(2,1)}, u32[]{:S(2)}, u32[]{:S(2)}) async-start(bf16[16,1,64,256]{3,2,1,0:T(8,128)(2,1)} %copy.103), calls=%async_computation.3 | async-start | bytes 1048576 | tf_op jit(solution)/shard_map/all_to_all | solution.py:48
  410.9 17.3 %copy-start.4 = (f32[256,2]{0,1:T(2,128)S(1)}, f32[256,2]{0,1:T(2,128)}, u32[]{:S(2)}) copy-start(f32[256,2]{0,1:T(2,128)} %param.9) | copy-start | bytes 6148
  416.1 21.3 %all-to-all-start.6 = ((bf16[8,256,128]{2,1,0:T(8,128)(2,1)}), bf16[8,256,128]{2,1,0:T(8,128)(2,1)}, u32[]{:S(2)}, u32[]{:S(2)}) async-start(bf16[8,256,128]{2,1,0:T(8,128)(2,1)} %fusion.7), calls=%async_computation.6 | async-start | bytes 1048576 | tf_op jit(solution)/shard_map/all_to_all | solution.py:88
  438.6 3.0 copy-start.1
Sparse Core Ops, SparseCore 0:
  294.9 105.5 all-gather.1
